TPU v7x, 32 devices: a whole 2x2x4 slice. The times are simulated.
32 devices in a mesh: fs: 4 (over z), rep: 4 (over y, x), tp: 2 (over core).
Axes of the slice: x: 2, y: 2, z: 4, core: 2. Of those that a mesh axis runs over, the one named last changes fastest.
Arguments:
- saved_input: bfloat16 [16384, 2048], P(('fs', 'rep')), may hold values from -6 to 6
- cot_input: bfloat16 [16384, 1024], P(('fs', 'rep'), 'tp'), may hold values from -0.046875 to 0.046875
- cot_gate: bfloat16 [16384, 1024], P(('fs', 'rep'), 'tp'), may hold values from -0.046875 to 0.046875
- in_master: float32 [2048, 1024], P('fs', 'tp'), may hold values from -3 to 3
- gate_master: float32 [2048, 1024], P('fs', 'tp'), may hold values from -3 to 3
- in_factor: bfloat16 [2048, 256], P('fs'), may hold values from -0.125 to 0.125
- gate_factor: bfloat16 [2048, 256], P('fs'), may hold values from -0.125 to 0.125
- in_first: float32 [256, 1024], P('fs', 'tp'), may hold values from -6 to 6
- in_second: float32 [256, 1024], P('fs', 'tp'), may hold values from 0.5 to 2
- gate_first: float32 [256, 1024], P('fs', 'tp'), may hold values from -6 to 6
- gate_second: float32 [256, 1024], P('fs', 'tp'), may hold values from 0.5 to 2
Outputs:
- in_master_new: float32 [2048, 1024], P('fs', 'tp')
- gate_master_new: float32 [2048, 1024], P('fs', 'tp')
- in_update: float32 [2048, 1024], P('fs', 'tp')
- gate_update: float32 [2048, 1024], P('fs', 'tp')
- in_first_new: float32 [256, 1024], P('fs', 'tp')
- in_second_new: float32 [256, 1024], P('fs', 'tp')
- gate_first_new: float32 [256, 1024], P('fs', 'tp')
- gate_second_new: float32 [256, 1024], P('fs', 'tp')
- in_copy: bfloat16 [2048, 1024], P(None, 'tp')
- gate_copy: bfloat16 [2048, 1024], P(None, 'tp')
All inputs are finite; a program needn't handle non-finite values.
Results may differ from a plain program's by a relative error of at most 0.0065.
Values may be sent and summed in bfloat16 or wider, within the bound.
No kernel may reach another device: no remote copies, remote signals or barrier semaphores. Data moves between devices by JAX's collectives and lax.ppermute only.
A program may use at most 64 MiB of HBM per device.

v0:
```python
import jax
import jax.numpy as jnp
from jax import lax
from jax.sharding import PartitionSpec as P

D = 2048
W = 1024
CONTRACT_ROWS = (((0,), (0,)), ((), ()))


def plain_rows(left, right):
    return lax.dot_general(left, right, CONTRACT_ROWS, preferred_element_type=jnp.float32)


def split_parts(values):
    upper = values.astype(jnp.bfloat16)
    lower = (values - upper.astype(jnp.float32)).astype(jnp.bfloat16)
    return (upper, lower)


def on_device(
    saved_input,
    cot_input,
    cot_gate,
    in_master,
    gate_master,
    in_factor,
    gate_factor,
    in_first,
    in_second,
    gate_first,
    gate_second,
):
    width = in_master.shape[1]
    in_basis = in_factor.astype(jnp.float32)
    gate_basis = gate_factor.astype(jnp.float32)
    in_whole, gate_whole = (
        lax.all_gather(in_factor, "fs", axis=0, tiled=True),
        lax.all_gather(gate_factor, "fs", axis=0, tiled=True),
    )
    in_upper, in_lower = split_parts(
        jnp.dot(saved_input, in_whole, preferred_element_type=jnp.float32)
    )
    gate_upper, gate_lower = split_parts(
        jnp.dot(saved_input, gate_whole, preferred_element_type=jnp.float32)
    )
    left = plain_rows(in_upper, cot_input)
    left = left + plain_rows(in_lower, cot_input)
    right = plain_rows(gate_upper, cot_gate)
    right = right + plain_rows(gate_lower, cot_gate)
    partial_low = lax.psum_scatter(
        jnp.concatenate([left, right], axis=1).astype(jnp.bfloat16),
        "fs",
        scatter_dimension=0,
        tiled=True,
    )
    low = lax.psum(partial_low, "rep").astype(jnp.float32)
    first_old = jnp.concatenate([in_first, gate_first], axis=1)
    second_old = jnp.concatenate([in_second, gate_second], axis=1)
    first_new = 0.8 * first_old + 0.2 * low
    second_new = 0.95 * second_old + 0.05 * low * low
    normed = first_new / jnp.sqrt(second_new)
    piece = lax.all_gather(normed, "fs", axis=0, tiled=True)
    left = jnp.dot(in_basis, piece[:, :width], precision=lax.Precision.HIGHEST)
    right = jnp.dot(gate_basis, piece[:, width:], precision=lax.Precision.HIGHEST)
    in_square, gate_square = lax.psum((jnp.sum(left * left), jnp.sum(right * right)), ("fs", "tp"))
    in_update = left / jnp.sqrt(in_square / (D * W) + 0.1)
    gate_update = right / jnp.sqrt(gate_square / (D * W) + 0.1)
    in_master_new = in_master - 0.05 * in_update
    gate_master_new = gate_master - 0.05 * gate_update
    in_copy, gate_copy = (
        lax.all_gather(in_master_new.astype(jnp.bfloat16), "fs", axis=0, tiled=True),
        lax.all_gather(gate_master_new.astype(jnp.bfloat16), "fs", axis=0, tiled=True),
    )
    return (
        in_master_new,
        gate_master_new,
        in_update,
        gate_update,
        first_new[:, :width],
        second_new[:, :width],
        first_new[:, width:],
        second_new[:, width:],
        in_copy,
        gate_copy,
    )


def solution(mesh):
    placed = (
        P(("fs", "rep"), None),
        P(("fs", "rep"), "tp"),
        P(("fs", "rep"), "tp"),
        P("fs", "tp"),
        P("fs", "tp"),
        P("fs", None),
        P("fs", None),
        P("fs", "tp"),
        P("fs", "tp"),
        P("fs", "tp"),
        P("fs", "tp"),
    )
    return jax.shard_map(
        on_device,
        mesh=mesh,
        in_specs=placed,
        out_specs=(
            P("fs", "tp"),
            P("fs", "tp"),
            P("fs", "tp"),
            P("fs", "tp"),
            P("fs", "tp"),
            P("fs", "tp"),
            P("fs", "tp"),
            P("fs", "tp"),
            P(None, "tp"),
            P(None, "tp"),
        ),
        check_vma=False,
    )
```

profile of v0, /device:TPU:0, one launch (start us, length us, event | category | flops | bytes accessed | tf_op | source)
XLA Modules:
  0.0 296.7 jit_solution(4529653988439130760)
XLA Ops:
  8.7 31.6 %all-gather.8.cloned.1.call-done = bf16[2048,256]{1,0:T(8,128)(2,1)} async-done(((bf16[512,256]{1,0:T(8,128)(2,1)}), bf16[2048,256]{1,0:T(8,128)(2,1)}) %all-gather.8.cloned.1.call-update) | async-done | bytes 1048592 | tf_op jit(solution)/shard_map/all_gather | solution.py:39
  40.3 3.7 %fusion.21 = f32[1024,256]{1,0:T(8,128)S(1)} fusion(bf16[1024,2048]{1,0:T(8,128)(2,1)} %param.11, bf16[2048,256]{1,0:T(8,128)(2,1)} %all-gather.8.cloned.1.call-done), kind=kOutput, calls=%fused_computation.35 | convolution fusion | flops 1073741824 | bytes 6291456 | tf_op jit(solution)/shard_map/dot_general | solution.py:45
  45.8 23.5 %all-gather.6.cloned.1.call-done = bf16[2048,256]{1,0:T(8,128)(2,1)} async-done(((bf16[512,256]{1,0:T(8,128)(2,1)}), bf16[2048,256]{1,0:T(8,128)(2,1)}) %all-gather.6.cloned.1.call-update) | async-done | bytes 1048592 | tf_op jit(solution)/shard_map/all_gather | solution.py:38
  69.3 3.7 %fusion.20 = f32[1024,256]{1,0:T(8,128)S(1)} fusion(bf16[1024,2048]{1,0:T(8,128)(2,1)} %param.11, bf16[2048,256]{1,0:T(8,128)(2,1)} %all-gather.6.cloned.1.call-done), kind=kOutput, calls=%fused_computation.34 | convolution fusion | flops 1073741824 | bytes 6291456 | tf_op jit(solution)/shard_map/dot_general | solution.py:42
  75.0 21.3 %reduce-scatter.2.cloned.1.call-done = bf16[64,1024]{1,0:T(8,128)(2,1)} async-done(((bf16[256,1024]{1,0:T(8,128)(2,1)}), bf16[64,1024]{1,0:T(8,128)(2,1)}) %reduce-scatter.2.cloned.1.call-update) | async-done | bytes 131088 | tf_op jit(solution)/shard_map/reduce_scatter | solution.py:51
  96.4 43.2 %all-reduce.3.cloned.1.call-done = bf16[64,1024]{1,0:T(8,128)(2,1)} async-done(((bf16[64,1024]{1,0:T(8,128)(2,1)}), bf16[64,1024]{1,0:T(8,128)(2,1)}) %all-reduce.3.cloned.1.call-update) | async-done | bytes 131088 | tf_op jit(solution)/shard_map/psum | solution.py:57
  139.6 2.0 rsqrt_multiply_fusion
  141.7 1.3 copy.21
  143.0 26.8 %all-gather.10.cloned.1.call-done = f32[256,1024]{1,0:T(8,128)} async-done(((f32[64,1024]{1,0:T(8,128)}), f32[256,1024]{1,0:T(8,128)}) %all-gather.10.cloned.1.call-update) | async-done | bytes 1048592 | tf_op jit(solution)/shard_map/all_gather | solution.py:63
  169.8 3.6 %multiply_reduce_fusion = (f32[]{:T(128)}, f32[512,512]{1,0:T(8,128)}) fusion(bf16[512,256]{1,0:T(8,128)(2,1)S(1)} %copy-done.3, f32[256,1024]{1,0:T(8,128)} %all-gather.10.cloned.1.call-done), kind=kOutput, calls=%fused_computation.6 | convolution fusion | flops 805830656 | bytes 1835012 | tf_op jit(solution)/shard_map/dot_general | solution.py:65
  173.4 3.6 %multiply_reduce_fusion.1 = (f32[]{:T(128)}, f32[512,512]{1,0:T(8,128)}) fusion(bf16[512,256]{1,0:T(8,128)(2,1)S(1)} %copy-done.4, f32[256,1024]{1,0:T(8,128)} %all-gather.10.cloned.1.call-done), kind=kOutput, calls=%fused_computation.9 | convolution fusion | flops 805830656 | bytes 1835012 | tf_op jit(solution)/shard_map/dot_general | solution.py:64
  177.0 15.3 %all-reduce = (f32[]{:T(128)}, f32[]{:T(128)}) all-reduce(f32[]{:T(128)} %get-tuple-element.35, f32[]{:T(128)} %get-tuple-element.37), channel_id=1, replica_groups=mesh['fs'=4,'rep'=4,'tp'=2] {'fs','tp'}, use_global_device_ids=true, to_apply=%region_3.0 | all-reduce | flops 2 | bytes 16 | tf_op jit(solution)/shard_map/psum | solution.py:66
  193.0 2.7 fusion.15
  195.7 2.5 copy.22
  199.0 3.4 %fusion.14 = (bf16[512,512]{0,1:T(8,128)(2,1)}, f32[512,512]{0,1:T(8,128)}, f32[512,512]{0,1:T(8,128)}) fusion(f32[512,512]{0,1:T(8,128)} %copy.22, f32[512,512]{1,0:T(8,128)} %get-tuple-element.38, f32[]{:T(128)S(6)} %sqrt.11), kind=kLoop, calls=%fused_computation.30 | loop fusion | flops 1048576 | bytes 4718596 | tf_op jit(solution)/shard_map/convert_element_type | solution.py:73
  202.4 1.8 fusion.18
  204.2 2.5 copy.24
  206.7 2.5 copy.26
  209.3 1.3 copy.23
  210.6 1.3 copy.25
  211.9 28.0 %all-gather.12.cloned.1.call-done = bf16[2048,512]{0,1:T(8,128)(2,1)} async-done(((bf16[512,512]{0,1:T(8,128)(2,1)}), bf16[2048,512]{0,1:T(8,128)(2,1)}) %all-gather.12.cloned.1.call-update) | async-done | bytes 2097168 | tf_op jit(solution)/shard_map/all_gather | solution.py:72
  239.9 3.9 %copy.27 = bf16[2048,512]{1,0:T(8,128)(2,1)} copy(bf16[2048,512]{0,1:T(8,128)(2,1)} %all-gather.12.cloned.1.call-done) | data formatting | bytes 4194304
  243.8 42.1 %all-gather.14.cloned.1.call-done = bf16[2048,512]{0,1:T(8,128)(2,1)} async-done(((bf16[512,512]{0,1:T(8,128)(2,1)}), bf16[2048,512]{0,1:T(8,128)(2,1)}) %all-gather.14.cloned.1.call-update) | async-done | bytes 2097168 | tf_op jit(solution)/shard_map/all_gather | solution.py:73
  285.9 3.9 %copy.28 = bf16[2048,512]{1,0:T(8,128)(2,1)} copy(bf16[2048,512]{0,1:T(8,128)(2,1)} %all-gather.14.cloned.1.call-done) | data formatting | bytes 4194304
  (35 shorter events, 5.3 us)
Async XLA Ops:
  7.2 36.9 %copy-start = (bf16[1024,512]{1,0:T(8,128)(2,1)S(1)}, bf16[1024,512]{1,0:T(8,128)(2,1)}, u32[]{:S(2)}) copy-start(bf16[1024,512]{1,0:T(8,128)(2,1)} %param.13) | copy-start | bytes 3145732
  7.2 33.1 %all-gather.8.cloned.1.call-start = ((), (), s32[]{:S(2)}) async-start(), calls=%async_computation.2 | async-start | bytes 1310720 | tf_op jit(solution)/shard_map/all_gather | solution.py:39
  7.9 61.3 %all-gather.6.cloned.1.call-start = ((), (), s32[]{:S(2)}) async-start(), calls=%async_computation.1 | async-start | bytes 1310720 | tf_op jit(solution)/shard_map/all_gather | solution.py:38
  8.7 87.6 %reduce-scatter.2.cloned.1.call-start = ((), (), s32[]{:S(2)}) async-start(), calls=%async_computation.3 | async-start | bytes 655360 | tf_op jit(solution)/shard_map/reduce_scatter | solution.py:51
  45.8 27.3 %copy-start.1 = (bf16[1024,512]{1,0:T(8,128)(2,1)S(1)}, bf16[1024,512]{1,0:T(8,128)(2,1)}, u32[]{:S(2)}) copy-start(bf16[1024,512]{1,0:T(8,128)(2,1)} %param.12) | copy-start | bytes 3145732
  73.0 1.0 copy-start.6
  73.0 66.5 %copy-start.7 = (f32[64,512]{1,0:T(8,128)S(1)}, f32[64,512]{1,0:T(8,128)}, u32[]{:S(2)}) copy-start(f32[64,512]{1,0:T(8,128)} %param.21) | copy-start | bytes 393220
  73.0 68.6 %copy-start.2 = (f32[512,512]{1,0:T(8,128)S(1)}, f32[512,512]{1,0:T(8,128)}, u32[]{:S(2)}) copy-start(f32[512,512]{1,0:T(8,128)} %param.14) | copy-start | bytes 3145732
  73.5 96.2 %copy-start.3 = (bf16[512,256]{1,0:T(8,128)(2,1)S(1)}, bf16[512,256]{1,0:T(8,128)(2,1)}, u32[]{:S(2)}) copy-start(bf16[512,256]{1,0:T(8,128)(2,1)} %param.17) | copy-start | bytes 786436
  74.1 99.3 %copy-start.4 = (bf16[512,256]{1,0:T(8,128)(2,1)S(1)}, bf16[512,256]{1,0:T(8,128)(2,1)}, u32[]{:S(2)}) copy-start(bf16[512,256]{1,0:T(8,128)(2,1)} %param.16) | copy-start | bytes 786436
  75.0 64.6 %all-reduce.3.cloned.1.call-start = ((), (), s32[]{:S(2)}) async-start(), calls=%async_computation.4 | async-start | bytes 262144 | tf_op jit(solution)/shard_map/psum | solution.py:57
  96.3 73.4 %all-gather.10.cloned.1.call-start = ((), (), s32[]{:S(2)}) async-start(), calls=%async_computation.5 | async-start | bytes 1310720 | tf_op jit(solution)/shard_map/all_gather | solution.py:63
  141.6 98.2 %all-gather.12.cloned.1.call-start = ((), (), s32[]{:S(2)}) async-start(), calls=%async_computation.6 | async-start | bytes 2621440 | tf_op jit(solution)/shard_map/all_gather | solution.py:72
  195.7 6.7 %copy-start.5 = (f32[64,1024]{1,0:T(8,128)S(1)}, f32[64,1024]{1,0:T(8,128)}, u32[]{:S(2)}) copy-start(f32[64,1024]{1,0:T(8,128)} %get-tuple-element.29) | copy-start | bytes 786436
  195.7 90.2 %all-gather.14.cloned.1.call-start = ((), (), s32[]{:S(2)}) async-start(), calls=%async_computation.7 | async-start | bytes 2621440 | tf_op jit(solution)/shard_map/all_gather | solution.py:73
Sparse Core Ops, SparseCore 0:
  9.6 30.6 all-gather.7
  41.9 27.3 all-gather.5
  75.1 21.1 reduce-scatter.1
  99.1 40.4 all-reduce.2
  141.7 27.9 all-gather.9
  195.8 44.0 all-gather.11
  241.4 44.4 all-gather.13
where the time goes:
time: 297 us
  waiting for transfers between devices  218 us (73%)
  local copies, waits for them, and re-layouts  21.2 us (7%)
  matrix products  17.3 us (6%)
  between operations  15.7 us (5%)
  blocking collectives  15.3 us (5%)
  other arithmetic  8.96 us (3%)
    psum x1, waiting for transfers between devices, on_device(): low = lax.psum(partial_low, 'rep').astype(jnp.float32)  43.2 us
    all_gather x1, waiting for transfers between devices, on_device(): lax.all_gather(gate_master_new.astype(jnp.bfloat16), 'fs', axis=0, tiled=...  42.1 us
    all_gather x1, waiting for transfers between devices, on_device(): lax.all_gather(gate_factor, 'fs', axis=0, tiled=True)  31.6 us
    all_gather x1, waiting for transfers between devices, on_device(): lax.all_gather(in_master_new.astype(jnp.bfloat16), 'fs', axis=0, tiled=True)  28 us
    all_gather x1, waiting for transfers between devices, on_device(): piece = lax.all_gather(normed, 'fs', axis=0, tiled=True)  26.8 us
    all_gather x1, waiting for transfers between devices, on_device(): lax.all_gather(in_factor, 'fs', axis=0, tiled=True)  23.5 us
    reduce_scatter x1, waiting for transfers between devices, on_device(): lax.psum_scatter(jnp.concatenate([left, right], axis=1).astype(jnp.bfloat...  21.3 us
    unnamed x24, local copies, waits for them, and re-layouts  19.4 us
  transfers between devices with their start and end apart: 7, of which 7 were waited for; matrix products, arithmetic and copies ran while one was open for 9% of the time, Pallas kernels for 0%

commit v1 on v0

--- a/solution.py
+++ b/solution.py
@@ -54,7 +54,7 @@
         scatter_dimension=0,
         tiled=True,
     )
-    low = lax.psum(partial_low, "rep").astype(jnp.float32)
+    low = jnp.sum(lax.all_gather(partial_low, "rep"), axis=0).astype(jnp.float32)
     first_old = jnp.concatenate([in_first, gate_first], axis=1)
     second_old = jnp.concatenate([in_second, gate_second], axis=1)
     first_new = 0.8 * first_old + 0.2 * low

time: 297 us -> 262 us (0.88)
  waiting for transfers between devices: 218 us -> 172 us
  blocking collectives: 15.3 us -> 26.3 us
    psum x1 -> x0, waiting for transfers between devices: 43.2 us -> none  [on_device(): low = lax.psum(partial_low, 'rep').astype(jnp.float32)]
    all_gather x0 -> x1, blocking collectives: none -> 11 us  [on_device(): lax.all_gather(partial_low, 'rep')]
  transfers between devices with their start and end apart: 7 -> 6, of which waited for: 7 -> 6; matrix products, arithmetic and copies ran while one was open for 9% -> 10% of each run, Pallas kernels for 0% -> 0%
where the time goes in v1:
time: 262 us
  waiting for transfers between devices  172 us (66%)
  blocking collectives  26.3 us (10%)
  local copies, waits for them, and re-layouts  21.2 us (8%)
  matrix products  17.3 us (7%)
  between operations  15.7 us (6%)
  other arithmetic  8.99 us (3%)
    all_gather x1, waiting for transfers between devices, on_device(): lax.all_gather(gate_master_new.astype(jnp.bfloat16), 'fs', axis=0, tiled=...  42 us
    all_gather x1, waiting for transfers between devices, on_device(): lax.all_gather(gate_factor, 'fs', axis=0, tiled=True)  31.6 us
    all_gather x1, waiting for transfers between devices, on_device(): lax.all_gather(in_master_new.astype(jnp.bfloat16), 'fs', axis=0, tiled=True)  28 us
    all_gather x1, waiting for transfers between devices, on_device(): piece = lax.all_gather(normed, 'fs', axis=0, tiled=True)  24.2 us
    all_gather x1, waiting for transfers between devices, on_device(): lax.all_gather(in_factor, 'fs', axis=0, tiled=True)  23.5 us
    reduce_scatter x1, waiting for transfers between devices, on_device(): lax.psum_scatter(jnp.concatenate([left, right], axis=1).astype(jnp.bfloat...  21.3 us
    unnamed x24, local copies, waits for them, and re-layouts  19.4 us
    psum x1, blocking collectives, on_device(): lax.psum((jnp.sum(left * left), jnp.sum(right * right)), ('fs', 'tp'))  15.3 us
  transfers between devices with their start and end apart: 6, of which 6 were waited for; matrix products, arithmetic and copies ran while one was open for 10% of the time, Pallas kernels for 0%

profile of v1, /device:TPU:0, one launch (start us, length us, event | category | flops | bytes accessed | tf_op | source)
XLA Modules:
  0.0 261.7 jit_solution(11503713809066541637)
XLA Ops:
  8.7 31.6 %all-gather.9.cloned.1.call-done = bf16[2048,256]{1,0:T(8,128)(2,1)} async-done(((bf16[512,256]{1,0:T(8,128)(2,1)}), bf16[2048,256]{1,0:T(8,128)(2,1)}) %all-gather.9.cloned.1.call-update) | async-done | bytes 1048592 | tf_op jit(solution)/shard_map/all_gather | solution.py:39
  40.3 3.7 %fusion.21 = f32[1024,256]{1,0:T(8,128)S(1)} fusion(bf16[1024,2048]{1,0:T(8,128)(2,1)} %param.11, bf16[2048,256]{1,0:T(8,128)(2,1)} %all-gather.9.cloned.1.call-done), kind=kOutput, calls=%fused_computation.35 | convolution fusion | flops 1073741824 | bytes 6291456 | tf_op jit(solution)/shard_map/dot_general | solution.py:45
  45.8 23.5 %all-gather.7.cloned.1.call-done = bf16[2048,256]{1,0:T(8,128)(2,1)} async-done(((bf16[512,256]{1,0:T(8,128)(2,1)}), bf16[2048,256]{1,0:T(8,128)(2,1)}) %all-gather.7.cloned.1.call-update) | async-done | bytes 1048592 | tf_op jit(solution)/shard_map/all_gather | solution.py:38
  69.3 3.7 %fusion.20 = f32[1024,256]{1,0:T(8,128)S(1)} fusion(bf16[1024,2048]{1,0:T(8,128)(2,1)} %param.11, bf16[2048,256]{1,0:T(8,128)(2,1)} %all-gather.7.cloned.1.call-done), kind=kOutput, calls=%fused_computation.34 | convolution fusion | flops 1073741824 | bytes 6291456 | tf_op jit(solution)/shard_map/dot_general | solution.py:42
  75.0 21.3 %reduce-scatter.2.cloned.1.call-done = bf16[64,1024]{1,0:T(8,128)(2,1)} async-done(((bf16[256,1024]{1,0:T(8,128)(2,1)}), bf16[64,1024]{1,0:T(8,128)(2,1)}) %reduce-scatter.2.cloned.1.call-update) | async-done | bytes 131088 | tf_op jit(solution)/shard_map/reduce_scatter | solution.py:51
  96.4 11.0 %all-gather = bf16[256,1024]{1,0:T(8,128)(2,1)S(1)} all-gather(bf16[64,1024]{1,0:T(8,128)(2,1)} %reduce-scatter.2.cloned.1.call-done), channel_id=2, replica_groups=mesh['fs'=4,'rep'=4,'tp'=2] {'rep'}, dimensions={0}, use_global_device_ids=true | all-gather | bytes 655360 | tf_op jit(solution)/shard_map/all_gather | solution.py:57
  107.4 2.0 rsqrt_multiply_fusion
  109.5 1.3 copy.21
  110.8 24.2 %all-gather.11.cloned.1.call-done = f32[256,1024]{1,0:T(8,128)} async-done(((f32[64,1024]{1,0:T(8,128)}), f32[256,1024]{1,0:T(8,128)}) %all-gather.11.cloned.1.call-update) | async-done | bytes 1048592 | tf_op jit(solution)/shard_map/all_gather | solution.py:63
  134.9 3.6 %multiply_reduce_fusion = (f32[]{:T(128)}, f32[512,512]{1,0:T(8,128)}) fusion(bf16[512,256]{1,0:T(8,128)(2,1)S(1)} %copy-done.3, f32[256,1024]{1,0:T(8,128)} %all-gather.11.cloned.1.call-done), kind=kOutput, calls=%fused_computation.6 | convolution fusion | flops 805830656 | bytes 1835012 | tf_op jit(solution)/shard_map/dot_general | solution.py:65
  138.6 3.6 %multiply_reduce_fusion.1 = (f32[]{:T(128)}, f32[512,512]{1,0:T(8,128)}) fusion(bf16[512,256]{1,0:T(8,128)(2,1)S(1)} %copy-done.4, f32[256,1024]{1,0:T(8,128)} %all-gather.11.cloned.1.call-done), kind=kOutput, calls=%fused_computation.9 | convolution fusion | flops 805830656 | bytes 1835012 | tf_op jit(solution)/shard_map/dot_general | solution.py:64
  142.2 15.3 %all-reduce = (f32[]{:T(128)}, f32[]{:T(128)}) all-reduce(f32[]{:T(128)} %get-tuple-element.35, f32[]{:T(128)} %get-tuple-element.37), channel_id=1, replica_groups=mesh['fs'=4,'rep'=4,'tp'=2] {'fs','tp'}, use_global_device_ids=true, to_apply=%region_3.0 | all-reduce | flops 2 | bytes 16 | tf_op jit(solution)/shard_map/psum | solution.py:66
  158.2 2.7 %fusion.15 = (bf16[512,512]{0,1:T(8,128)(2,1)}, f32[512,512]{0,1:T(8,128)S(1)}, f32[512,512]{0,1:T(8,128)S(1)}) fusion(f32[512,512]{0,1:T(8,128)} %copy.21, f32[512,512]{1,0:T(8,128)} %get-tuple-element.36, f32[]{:T(128)S(6)} %sqrt.10), kind=kLoop, calls=%fused_computation.31 | loop fusion | flops 1048576 | bytes 4718596 | tf_op jit(solution)/shard_map/convert_element_type | solution.py:72
  160.9 2.5 copy.22
  164.1 3.4 %fusion.14 = (bf16[512,512]{0,1:T(8,128)(2,1)}, f32[512,512]{0,1:T(8,128)}, f32[512,512]{0,1:T(8,128)}) fusion(f32[512,512]{0,1:T(8,128)} %copy.22, f32[512,512]{1,0:T(8,128)} %get-tuple-element.38, f32[]{:T(128)S(6)} %sqrt.11), kind=kLoop, calls=%fused_computation.30 | loop fusion | flops 1048576 | bytes 4718596 | tf_op jit(solution)/shard_map/convert_element_type | solution.py:73
  167.6 1.8 fusion.18
  169.4 2.5 copy.24
  171.9 2.5 copy.26
  174.4 1.3 copy.23
  175.7 1.3 copy.25
  177.1 28.0 %all-gather.13.cloned.1.call-done = bf16[2048,512]{0,1:T(8,128)(2,1)} async-done(((bf16[512,512]{0,1:T(8,128)(2,1)}), bf16[2048,512]{0,1:T(8,128)(2,1)}) %all-gather.13.cloned.1.call-update) | async-done | bytes 2097168 | tf_op jit(solution)/shard_map/all_gather | solution.py:72
  205.0 3.9 %copy.27 = bf16[2048,512]{1,0:T(8,128)(2,1)} copy(bf16[2048,512]{0,1:T(8,128)(2,1)} %all-gather.13.cloned.1.call-done) | data formatting | bytes 4194304
  208.9 42.0 %all-gather.15.cloned.1.call-done = bf16[2048,512]{0,1:T(8,128)(2,1)} async-done(((bf16[512,512]{0,1:T(8,128)(2,1)}), bf16[2048,512]{0,1:T(8,128)(2,1)}) %all-gather.15.cloned.1.call-update) | async-done | bytes 2097168 | tf_op jit(solution)/shard_map/all_gather | solution.py:73
  251.0 3.9 %copy.28 = bf16[2048,512]{1,0:T(8,128)(2,1)} copy(bf16[2048,512]{0,1:T(8,128)(2,1)} %all-gather.15.cloned.1.call-done) | data formatting | bytes 4194304
  (34 shorter events, 5.3 us)
Async XLA Ops:
  7.2 36.9 %copy-start = (bf16[1024,512]{1,0:T(8,128)(2,1)S(1)}, bf16[1024,512]{1,0:T(8,128)(2,1)}, u32[]{:S(2)}) copy-start(bf16[1024,512]{1,0:T(8,128)(2,1)} %param.13) | copy-start | bytes 3145732
  7.2 33.1 %all-gather.9.cloned.1.call-start = ((), (), s32[]{:S(2)}) async-start(), calls=%async_computation.2 | async-start | bytes 1310720 | tf_op jit(solution)/shard_map/all_gather | solution.py:39
  7.9 61.3 %all-gather.7.cloned.1.call-start = ((), (), s32[]{:S(2)}) async-start(), calls=%async_computation.1 | async-start | bytes 1310720 | tf_op jit(solution)/shard_map/all_gather | solution.py:38
  8.7 87.7 %reduce-scatter.2.cloned.1.call-start = ((), (), s32[]{:S(2)}) async-start(), calls=%async_computation.3 | async-start | bytes 655360 | tf_op jit(solution)/shard_map/reduce_scatter | solution.py:51
  45.8 27.3 %copy-start.1 = (bf16[1024,512]{1,0:T(8,128)(2,1)S(1)}, bf16[1024,512]{1,0:T(8,128)(2,1)}, u32[]{:S(2)}) copy-start(bf16[1024,512]{1,0:T(8,128)(2,1)} %param.12) | copy-start | bytes 3145732
  73.0 1.0 copy-start.6
  73.0 34.4 %copy-start.7 = (f32[64,512]{1,0:T(8,128)S(1)}, f32[64,512]{1,0:T(8,128)}, u32[]{:S(2)}) copy-start(f32[64,512]{1,0:T(8,128)} %param.21) | copy-start | bytes 393220
  73.5 35.9 %copy-start.2 = (f32[512,512]{1,0:T(8,128)S(1)}, f32[512,512]{1,0:T(8,128)}, u32[]{:S(2)}) copy-start(f32[512,512]{1,0:T(8,128)} %param.14) | copy-start | bytes 3145732
  73.5 61.4 %copy-start.3 = (bf16[512,256]{1,0:T(8,128)(2,1)S(1)}, bf16[512,256]{1,0:T(8,128)(2,1)}, u32[]{:S(2)}) copy-start(bf16[512,256]{1,0:T(8,128)(2,1)} %param.17) | copy-start | bytes 786436
  74.1 64.5 %copy-start.4 = (bf16[512,256]{1,0:T(8,128)(2,1)S(1)}, bf16[512,256]{1,0:T(8,128)(2,1)}, u32[]{:S(2)}) copy-start(bf16[512,256]{1,0:T(8,128)(2,1)} %param.16) | copy-start | bytes 786436
  75.0 60.0 %all-gather.11.cloned.1.call-start = ((), (), s32[]{:S(2)}) async-start(), calls=%async_computation.4 | async-start | bytes 1310720 | tf_op jit(solution)/shard_map/all_gather | solution.py:63
  109.4 95.6 %all-gather.13.cloned.1.call-start = ((), (), s32[]{:S(2)}) async-start(), calls=%async_computation.5 | async-start | bytes 2621440 | tf_op jit(solution)/shard_map/all_gather | solution.py:72
  160.8 6.7 %copy-start.5 = (f32[64,1024]{1,0:T(8,128)S(1)}, f32[64,1024]{1,0:T(8,128)}, u32[]{:S(2)}) copy-start(f32[64,1024]{1,0:T(8,128)} %get-tuple-element.29) | copy-start | bytes 786436
  160.9 90.1 %all-gather.15.cloned.1.call-start = ((), (), s32[]{:S(2)}) async-start(), calls=%async_computation.6 | async-start | bytes 2621440 | tf_op jit(solution)/shard_map/all_gather | solution.py:73
Sparse Core Ops, SparseCore 0:
  9.6 30.6 all-gather.8
  41.9 27.3 all-gather.6
  75.1 21.2 reduce-scatter.1
  109.5 25.3 all-gather.10
  161.0 44.0 all-gather.12
  206.5 44.4 all-gather.14
